TPU v7x, 32 devices: a whole 2x2x4 slice. The times are simulated.
32 devices in a mesh: sp: 8 (over z, x), tp: 4 (over y, core).
Axes of the slice: x: 2, y: 2, z: 4, core: 2. Of those that a mesh axis runs over, the one named last changes fastest.
Arguments:
- layer_input: bfloat16 [8, 1536, 2048], P('sp', 'tp'), may hold values from -6 to 6
- input_gain: float32 [2048], replicated, may hold values from 0.1 to 1.9
- key_weight: bfloat16 [2048, 512], P('sp', 'tp'), may hold values from -0.125 to 0.125
- value_weight: bfloat16 [2048, 512], P('sp', 'tp'), may hold values from -0.125 to 0.125
- key_gain: float32 [128], replicated, may hold values from 0.1 to 1.9
- stop_shift: bfloat16 [8, 4, 1536], P('sp', None, 'tp'), may hold values from -20 to 0
- new_query: bfloat16 [8, 16, 128], P('sp', 'tp'), may hold values from -6 to 6
- query_gain: float32 [128], replicated, may hold values from 0.1 to 1.9
- out_gain: float32 [128], replicated, may hold values from 0.1 to 1.9
Outputs:
- key_cache: bfloat16 [8, 4, 1536, 128], P('sp', 'tp')
- value_cache: bfloat16 [8, 4, 1536, 128], P('sp', 'tp')
- shift_cache: bfloat16 [8, 4, 1536], P('sp', 'tp')
- first_read: bfloat16 [8, 16, 128], P('sp', 'tp')
All inputs are finite; a program needn't handle non-finite values.
Results may differ from a plain program's by a relative error of at most 0.013.
Values may be sent and summed in bfloat16 or wider, within the bound.
A program may use at most 64 MiB of HBM per device.

v0:
```python
import jax
import jax.numpy as jnp
from jax import lax
from jax.sharding import PartitionSpec as P

KVH = 4
epsilon = 1e-06


def row_norm(value_entries, scaling):
    return (
        value_entries
        * lax.rsqrt(jnp.mean(value_entries * value_entries, axis=-1, keepdims=True) + epsilon)
        * scaling
    )


def shards(
    layer_input,
    input_gain,
    key_weight,
    value_weight,
    key_gain,
    stop_shift,
    new_query,
    query_gain,
    out_gain,
):
    groups = lax.axis_size("tp")
    copies = groups // KVH
    row_count = layer_input.shape[1]
    head_size = new_query.shape[2]
    score_scale = 1.0 / head_size**0.5
    normed = row_norm(layer_input[0].astype(jnp.float32), input_gain).astype(jnp.bfloat16)
    stacked = jnp.stack((key_weight, value_weight), 0)
    full_depth = lax.all_gather(stacked, "sp", axis=1, tiled=True)
    projected = jnp.einsum(
        "rd,kdc->krc",
        normed,
        lax.all_gather(full_depth, "tp", axis=2, tiled=True),
        preferred_element_type=jnp.float32,
    )
    key_rows = row_norm(projected[0].reshape(row_count, KVH, head_size), key_gain).astype(
        jnp.bfloat16
    )
    value_rows = projected[1].reshape(row_count, KVH, head_size).astype(jnp.bfloat16)
    local_shift = stop_shift[0]
    key_slots = jnp.repeat(key_rows, copies, axis=1)
    value_slots = jnp.repeat(value_rows, copies, axis=1)
    shift_slots = jnp.repeat(local_shift.T, copies, axis=1)
    key_got, value_got, shift_got = (
        lax.all_to_all(key_slots, "tp", split_axis=1, concat_axis=0, tiled=True),
        lax.all_to_all(value_slots, "tp", split_axis=1, concat_axis=0, tiled=True),
        lax.all_to_all(shift_slots, "tp", split_axis=1, concat_axis=0, tiled=True),
    )
    key_line = key_got[:, 0, :]
    value_line = value_got[:, 0, :]
    shift_line = shift_got[:, 0]
    length = key_line.shape[0]
    query_rows = row_norm(new_query[0].astype(jnp.float32), query_gain).astype(jnp.bfloat16)
    scores = (
        jnp.einsum("qd,ld->ql", query_rows, key_line, preferred_element_type=jnp.float32)
        * score_scale
    )
    scores = scores + shift_line.astype(jnp.float32)[None, :]
    log_keep = jax.nn.log_sigmoid(-scores)
    inside = lax.cumsum(log_keep, axis=1, reverse=True) - log_keep
    weights = jnp.exp(jax.nn.log_sigmoid(scores) + inside).astype(jnp.bfloat16)
    read_sum = jnp.dot(weights, value_line, preferred_element_type=jnp.float32)
    first_out = row_norm(read_sum, out_gain).astype(jnp.bfloat16)
    return (
        key_line.reshape(1, 1, length, head_size),
        value_line.reshape(1, 1, length, head_size),
        shift_line.reshape(1, 1, length),
        first_out[None],
    )


def solution(mesh):
    placed = (
        P("sp", "tp", None),
        P(),
        P("sp", "tp"),
        P("sp", "tp"),
        P(),
        P("sp", None, "tp"),
        P("sp", "tp", None),
        P(),
        P(),
    )
    return jax.shard_map(
        shards,
        mesh=mesh,
        in_specs=placed,
        out_specs=(
            P("sp", "tp", None, None),
            P("sp", "tp", None, None),
            P("sp", "tp", None),
            P("sp", "tp", None),
        ),
        check_vma=False,
    )
```

profile of v0, /device:TPU:0, one launch (start us, length us, event | category | flops | bytes accessed | tf_op | source)
XLA Modules:
  0.0 125.1 jit_solution(7521093562815016131)
XLA Ops:
  7.2 1.0 copy.25
  8.3 0.9 copy.26
  9.2 0.7 pad_maximum_fusion
  10.0 42.8 %all-gather.3.cloned.1.call-done = bf16[2,2048,128]{1,2,0:T(8,128)(2,1)} async-done(((bf16[2,256,128]{1,2,0:T(8,128)(2,1)}), bf16[2,2048,128]{1,2,0:T(8,128)(2,1)}) %all-gather.3.cloned.1.call-update) | async-done | bytes 1048592 | tf_op jit(solution)/shard_map/all_gather | solution.py:36
  52.8 0.7 copy.36
  53.5 0.5 broadcast.75
  54.0 0.7 reduce.5
  54.7 0.7 reshape.96
  55.3 3.2 %all-to-all-start.2 = ((bf16[4,2,192]{2,1,0:T(2,128)(2,1)}), bf16[4,2,192]{2,1,0:T(2,128)(2,1)S(1)}, u32[]{:S(2)}, u32[]{:S(2)}) async-start(bf16[4,2,192]{2,1,0:T(2,128)(2,1)} %reshape.96), calls=%async_computation.2 | async-start | bytes 8192 | tf_op jit(solution)/shard_map/all_to_all | solution.py:54
  58.6 0.8 fusion.22
  59.4 1.9 %fusion = f32[384]{0:T(512)S(1)} fusion(bf16[1,384,2048]{2,1,0:T(8,128)(2,1)} %param.9), kind=kLoop, calls=%fused_computation.2 | loop fusion | flops 2358912 | bytes 1574400 | tf_op jit(solution)/shard_map/reduce_sum | solution.py:13
  61.4 26.5 %all-gather.5.cloned.1.call-done = bf16[2,2048,512]{1,2,0:T(8,128)(2,1)} async-done(((bf16[2,2048,128]{1,2,0:T(8,128)(2,1)}), bf16[2,2048,512]{1,2,0:T(8,128)(2,1)}) %all-gather.5.cloned.1.call-update) | async-done | bytes 4194320 | tf_op jit(solution)/shard_map/all_gather | solution.py:40
  87.8 4.6 %fusion.10 = f32[2,384,512]{1,2,0:T(8,128)S(1)} fusion(bf16[2,2048,512]{1,2,0:T(8,128)(2,1)} %all-gather.5.cloned.1.call-done, bf16[1,384,2048]{2,1,0:T(8,128)(2,1)S(1)} %copy-done, f32[2048]{0:T(1024)S(1)} %copy-done.6, f32[384]{0:T(512)S(1)} %add_rsqrt_fusion.1), kind=kOutput, calls=%fused_computation.12 | convolution fusion | flops 1613758464 | bytes 7349760 | tf_op jit(solution)/shard_map/rd,kdc->krc/dot_general | solution.py:37
  92.6 0.3 copy.27
  92.9 0.2 copy-done.3
  93.1 1.0 multiply_convert_fusion
  94.1 3.5 %all-to-all-start = ((bf16[384,4,128]{2,0,1:T(8,128)(2,1)}), bf16[384,4,128]{2,0,1:T(8,128)(2,1)S(1)}, u32[]{:S(2)}, u32[]{:S(2)}) async-start(bf16[384,4,128]{2,0,1:T(8,128)(2,1)} %multiply_convert_fusion), calls=%async_computation | async-start | bytes 786432 | tf_op jit(solution)/shard_map/all_to_all | solution.py:52
  97.6 0.1 reshape.97
  97.8 0.9 copy.28
  98.7 6.3 %all-to-all-done = bf16[384,4,128]{2,0,1:T(8,128)(2,1)S(1)} async-done(((bf16[384,4,128]{2,0,1:T(8,128)(2,1)}), bf16[384,4,128]{2,0,1:T(8,128)(2,1)S(1)}, u32[]{:S(2)}, u32[]{:S(2)}) %all-to-all-start) | async-done | bytes 393248 | tf_op jit(solution)/shard_map/all_to_all | solution.py:52
  105.0 3.5 %all-to-all-start.1 = ((bf16[384,4,128]{2,0,1:T(8,128)(2,1)}), bf16[384,4,128]{2,0,1:T(8,128)(2,1)S(1)}, u32[]{:S(2)}, u32[]{:S(2)}) async-start(bf16[384,4,128]{2,0,1:T(8,128)(2,1)} %copy.28), calls=%async_computation.1 | async-start | bytes 786432 | tf_op jit(solution)/shard_map/all_to_all | solution.py:53
  108.5 0.3 fusion.17
  108.8 5.0 %reduce-window.6 = f32[4,12,128]{2,1,0:T(8,128)S(1)} reduce-window(f32[4,12,128]{2,1,0:T(8,128)S(1)} %reshape.89, f32[]{:T(128)} %constant.8.clone.1), window={size=1x1x128 pad=0_0x0_0x0_127}, to_apply=%region_3.4 | reduce-window | flops 780288 | bytes 49156 | tf_op jit(solution)/shard_map/reduce-window
  113.8 0.1 slice_reduce_fusion
  113.8 0.2 reduce-window.9
  114.0 0.1 slice.16
  114.1 0.1 add_bitcast_fusion
  114.2 1.6 %all-to-all-done.1 = bf16[384,4,128]{2,0,1:T(8,128)(2,1)S(1)} async-done(((bf16[384,4,128]{2,0,1:T(8,128)(2,1)}), bf16[384,4,128]{2,0,1:T(8,128)(2,1)S(1)}, u32[]{:S(2)}, u32[]{:S(2)}) %all-to-all-start.1) | async-done | bytes 393248 | tf_op jit(solution)/shard_map/all_to_all | solution.py:53
  115.8 0.3 multiply_reduce_fusion.1
  116.2 0.6 fusion.25
  116.8 0.7 copy.39
  117.5 0.7 copy.40
  (28 shorter events, 0.4 us)
Async XLA Ops:
  7.2 80.7 %copy-start = (bf16[1,384,2048]{2,1,0:T(8,128)(2,1)S(1)}, bf16[1,384,2048]{2,1,0:T(8,128)(2,1)}, u32[]{:S(2)}) copy-start(bf16[1,384,2048]{2,1,0:T(8,128)(2,1)} %param.9) | copy-start | bytes 4718596
  7.2 80.7 %copy-start.6 = (f32[2048]{0:T(1024)S(1)}, f32[2048]{0:T(1024)}, u32[]{:S(2)}) copy-start(f32[2048]{0:T(1024)} %param.10) | copy-start | bytes 24580
  7.2 45.6 %all-gather.3.cloned.1.call-start = ((), (), s32[]{:S(2)}) async-start(), calls=%async_computation.3 | async-start | bytes 1179648 | tf_op jit(solution)/shard_map/all_gather | solution.py:36
  9.9 77.9 %all-gather.5.cloned.1.call-start = ((), (), s32[]{:S(2)}) async-start(), calls=%async_computation.4 | async-start | bytes 5242880 | tf_op jit(solution)/shard_map/all_gather | solution.py:40
  55.3 38.8 %all-to-all-start.2 = ((bf16[4,2,192]{2,1,0:T(2,128)(2,1)}), bf16[4,2,192]{2,1,0:T(2,128)(2,1)S(1)}, u32[]{:S(2)}, u32[]{:S(2)}) async-start(bf16[4,2,192]{2,1,0:T(2,128)(2,1)} %reshape.96), calls=%async_computation.2 | async-start | bytes 8192 | tf_op jit(solution)/shard_map/all_to_all | solution.py:54
  92.5 0.7 copy-start.3
  92.5 15.9 %copy-start.2 = (bf16[1,4,128]{2,1,0:T(4,128)(2,1)S(1)}, bf16[1,4,128]{2,1,0:T(4,128)(2,1)}, u32[]{:S(2)}) copy-start(bf16[1,4,128]{2,1,0:T(4,128)(2,1)} %param.15) | copy-start | bytes 3076
  92.5 15.9 %copy-start.4 = (f32[128]{0:T(128)S(1)}, f32[128]{0:T(128)}, u32[]{:S(2)}) copy-start(f32[128]{0:T(128)} %param.16) | copy-start | bytes 1540
  92.8 23.3 %copy-start.5 = (f32[128]{0:T(128)S(1)}, f32[128]{0:T(128)}, u32[]{:S(2)}) copy-start(f32[128]{0:T(128)} %param.17) | copy-start | bytes 1540
  94.1 10.8 %all-to-all-start = ((bf16[384,4,128]{2,0,1:T(8,128)(2,1)}), bf16[384,4,128]{2,0,1:T(8,128)(2,1)S(1)}, u32[]{:S(2)}, u32[]{:S(2)}) async-start(bf16[384,4,128]{2,0,1:T(8,128)(2,1)} %multiply_convert_fusion), calls=%async_computation | async-start | bytes 786432 | tf_op jit(solution)/shard_map/all_to_all | solution.py:52
  97.7 20.6 %copy-start.1 = (bf16[4,1,384]{2,1,0:T(2,128)(2,1)}, bf16[4,1,384]{2,1,0:T(2,128)(2,1)S(1)}, u32[]{:S(2)}) copy-start(bf16[4,1,384]{2,1,0:T(2,128)(2,1)S(1)} %reshape.97) | copy-start | bytes 9220
  105.0 10.8 %all-to-all-start.1 = ((bf16[384,4,128]{2,0,1:T(8,128)(2,1)}), bf16[384,4,128]{2,0,1:T(8,128)(2,1)S(1)}, u32[]{:S(2)}, u32[]{:S(2)}) async-start(bf16[384,4,128]{2,0,1:T(8,128)(2,1)} %copy.28), calls=%async_computation.1 | async-start | bytes 786432 | tf_op jit(solution)/shard_map/all_to_all | solution.py:53
Sparse Core Ops, SparseCore 0:
  10.6 42.1 all-gather.2
  54.3 33.4 all-gather.4
where the time goes:
time: 126 us; the launch traced here: 125 us
  waiting for transfers between devices  77.2 us (61%)
  between operations  14.2 us (11%)
  other arithmetic  11.1 us (9%)
  starting transfers between devices  10.2 us (8%)
  local copies, waits for them, and re-layouts  7.15 us (6%)
  matrix products  5.2 us (4%)
    all_gather x1, waiting for transfers between devices, shards(): full_depth = lax.all_gather(stacked, 'sp', axis=1, tiled=True)  42.8 us
    all_gather x1, waiting for transfers between devices, shards(): lax.all_gather(full_depth, 'tp', axis=2, tiled=True)  26.5 us
    all_to_all x1, waiting for transfers between devices, shards(): lax.all_to_all(key_slots, 'tp', split_axis=1, concat_axis=0, tiled=True)  6.25 us
    another operation x2, other arithmetic  5.17 us
    unnamed x21, local copies, waits for them, and re-layouts  4.98 us
    dot_general x1, matrix products, shards(): jnp.einsum('rd,kdc->krc', normed, lax.all_gather(full_depth, 'tp', axis=2...  4.62 us
    all_to_all x1, starting transfers between devices, shards(): lax.all_to_all(key_slots, 'tp', split_axis=1, concat_axis=0, tiled=True)  3.46 us
    all_to_all x1, starting transfers between devices, shards(): lax.all_to_all(value_slots, 'tp', split_axis=1, concat_axis=0, tiled=True)  3.46 us
  transfers between devices with their start and end apart: 5, of which 4 were waited for; matrix products, arithmetic and copies ran while one was open for 14% of the time, Pallas kernels for 0%

commit v1 on v0

--- a/solution.py
+++ b/solution.py
@@ -1,3 +1,4 @@
+import functools
 import jax
 import jax.numpy as jnp
 from jax import lax
@@ -5,6 +6,21 @@
 
 KVH = 4
 epsilon = 1e-06
+
+
+def lift_goods(w_in, bus_axis, ndim_at):
+    n_axis = lax.axis_size(bus_axis)
+    inbox = [(rr, (rr + 1) % n_axis) for rr in range(n_axis)]
+    tmp = [None] * n_axis
+    tmp[n_axis - 1] = w_in
+    for q in range(n_axis - 2, -1, -1):
+        tmp[q] = lax.ppermute(tmp[q + 1], bus_axis, inbox)
+    s_next = jnp.concatenate(tmp, axis=ndim_at)
+    opened = (lax.axis_index(bus_axis) + 1) * w_in.shape[ndim_at]
+    return jnp.roll(s_next, opened, axis=ndim_at)
+
+
+register_the_zone = functools.partial(lift_goods, bus_axis="sp", ndim_at=1)
 
 
 def row_norm(value_entries, scaling):
@@ -33,7 +49,7 @@
     score_scale = 1.0 / head_size**0.5
     normed = row_norm(layer_input[0].astype(jnp.float32), input_gain).astype(jnp.bfloat16)
     stacked = jnp.stack((key_weight, value_weight), 0)
-    full_depth = lax.all_gather(stacked, "sp", axis=1, tiled=True)
+    full_depth = register_the_zone(stacked)
     projected = jnp.einsum(
         "rd,kdc->krc",
         normed,

time: 126 us -> 138 us (1.095)
  waiting for transfers between devices: 77.2 us -> 88.3 us
  starting transfers between devices: 10.2 us -> 13.4 us
  other arithmetic: 11.1 us -> 8.25 us
    ppermute x0 -> x7, waiting for transfers between devices: none -> 53.7 us  [lift_goods(): tmp[q] = lax.ppermute(tmp[q + 1], bus_axis, inbox)]
    all_gather x1 -> x0, waiting for transfers between devices: 42.8 us -> none  [shards(): full_depth = lax.all_gather(stacked, 'sp', axis=1, tiled=True)]
    ppermute x0 -> x7, starting transfers between devices: none -> 3.04 us  [lift_goods(): tmp[q] = lax.ppermute(tmp[q + 1], bus_axis, inbox)]
    reduce_sum x3, other arithmetic: 2.82 us -> 0.57 us  [row_norm(): jnp.mean(value_entries * value_entries, axis=-1, keepdims=True) + epsilon]
    unnamed x21 -> x37, local copies, waits for them, and re-layouts: 4.98 us -> 5.07 us
  transfers between devices with their start and end apart: 5 -> 11, of which waited for: 4 -> 10; matrix products, arithmetic and copies ran while one was open for 14% -> 11% of each run, Pallas kernels for 0% -> 0%
where the time goes in v1:
time: 138 us; the launch traced here: 137 us
  waiting for transfers between devices  88.3 us (64%)
  between operations  14.4 us (10%)
  starting transfers between devices  13.4 us (10%)
  other arithmetic  8.25 us (6%)
  local copies, waits for them, and re-layouts  7.6 us (6%)
  matrix products  5.21 us (4%)
    ppermute x7, waiting for transfers between devices, lift_goods(): tmp[q] = lax.ppermute(tmp[q + 1], bus_axis, inbox)  53.7 us
    all_gather x1, waiting for transfers between devices, shards(): lax.all_gather(full_depth, 'tp', axis=2, tiled=True)  26.7 us
    all_to_all x1, waiting for transfers between devices, shards(): lax.all_to_all(key_slots, 'tp', split_axis=1, concat_axis=0, tiled=True)  6.25 us
    another operation x2, other arithmetic  5.17 us
    unnamed x37, local copies, waits for them, and re-layouts  5.07 us
    dot_general x1, matrix products, shards(): jnp.einsum('rd,kdc->krc', normed, lax.all_gather(full_depth, 'tp', axis=2...  4.62 us
    all_to_all x1, starting transfers between devices, shards(): lax.all_to_all(key_slots, 'tp', split_axis=1, concat_axis=0, tiled=True)  3.59 us
    all_to_all x1, starting transfers between devices, shards(): lax.all_to_all(value_slots, 'tp', split_axis=1, concat_axis=0, tiled=True)  3.46 us
  transfers between devices with their start and end apart: 11, of which 10 were waited for; matrix products, arithmetic and copies ran while one was open for 11% of the time, Pallas kernels for 0%

profile of v1, /device:TPU:0, one launch (start us, length us, event | category | flops | bytes accessed | tf_op | source)
XLA Modules:
  0.0 137.1 jit_solution(12285355865215490339)
XLA Ops:
  7.2 0.9 copy.25
  8.2 0.9 copy.26
  9.1 3.0 %collective-permute-start = (bf16[2,256,128]{1,2,0:T(8,128)(2,1)S(1)}, bf16[2,256,128]{1,2,0:T(8,128)(2,1)S(1)}, u32[]{:S(2)}, u32[]{:S(2)}) collective-permute-start(bf16[2,256,128]{1,2,0:T(8,128)(2,1)S(1)} %pad_maximum_fusion), channel_id=1, source_target_pairs={{0,4},{4,8},{8,12},{12,16},{16,20},{20,24},{24,28},{28,0},{1,5},{5... | collective-permute-start | bytes 393224 | tf_op jit(solution)/shard_map/ppermute | solution.py:17
  12.1 6.5 %collective-permute-done = bf16[2,256,128]{1,2,0:T(8,128)(2,1)S(1)} collective-permute-done((bf16[2,256,128]{1,2,0:T(8,128)(2,1)S(1)}, bf16[2,256,128]{1,2,0:T(8,128)(2,1)S(1)}, u32[]{:S(2)}, u32[]{:S(2)}) %collective-permute-start) | collective-permute-done | bytes 131104 | tf_op jit(solution)/shard_map/ppermute | solution.py:17
  18.7 7.7 %collective-permute-done.1 = bf16[2,256,128]{1,2,0:T(8,128)(2,1)S(1)} collective-permute-done((bf16[2,256,128]{1,2,0:T(8,128)(2,1)S(1)}, bf16[2,256,128]{1,2,0:T(8,128)(2,1)S(1)}, u32[]{:S(2)}, u32[]{:S(2)}) %collective-permute-start.1) | collective-permute-done | bytes 131104 | tf_op jit(solution)/shard_map/ppermute | solution.py:17
  26.3 7.7 %collective-permute-done.2 = bf16[2,256,128]{1,2,0:T(8,128)(2,1)S(1)} collective-permute-done((bf16[2,256,128]{1,2,0:T(8,128)(2,1)S(1)}, bf16[2,256,128]{1,2,0:T(8,128)(2,1)S(1)}, u32[]{:S(2)}, u32[]{:S(2)}) %collective-permute-start.2) | collective-permute-done | bytes 131104 | tf_op jit(solution)/shard_map/ppermute | solution.py:17
  34.0 7.7 %collective-permute-done.3 = bf16[2,256,128]{1,2,0:T(8,128)(2,1)S(1)} collective-permute-done((bf16[2,256,128]{1,2,0:T(8,128)(2,1)S(1)}, bf16[2,256,128]{1,2,0:T(8,128)(2,1)S(1)}, u32[]{:S(2)}, u32[]{:S(2)}) %collective-permute-start.3) | collective-permute-done | bytes 131104 | tf_op jit(solution)/shard_map/ppermute | solution.py:17
  41.7 7.7 %collective-permute-done.4 = bf16[2,256,128]{1,2,0:T(8,128)(2,1)S(1)} collective-permute-done((bf16[2,256,128]{1,2,0:T(8,128)(2,1)S(1)}, bf16[2,256,128]{1,2,0:T(8,128)(2,1)S(1)}, u32[]{:S(2)}, u32[]{:S(2)}) %collective-permute-start.4) | collective-permute-done | bytes 131104 | tf_op jit(solution)/shard_map/ppermute | solution.py:17
  49.4 8.9 %collective-permute-done.5 = bf16[2,256,128]{1,2,0:T(8,128)(2,1)S(1)} collective-permute-done((bf16[2,256,128]{1,2,0:T(8,128)(2,1)S(1)}, bf16[2,256,128]{1,2,0:T(8,128)(2,1)S(1)}, u32[]{:S(2)}, u32[]{:S(2)}) %collective-permute-start.5) | collective-permute-done | bytes 131104 | tf_op jit(solution)/shard_map/ppermute | solution.py:17
  58.2 7.7 %collective-permute-done.6 = bf16[2,256,128]{1,2,0:T(8,128)(2,1)S(1)} collective-permute-done((bf16[2,256,128]{1,2,0:T(8,128)(2,1)S(1)}, bf16[2,256,128]{1,2,0:T(8,128)(2,1)S(1)}, u32[]{:S(2)}, u32[]{:S(2)}) %collective-permute-start.6) | collective-permute-done | bytes 131104 | tf_op jit(solution)/shard_map/ppermute | solution.py:17
  66.2 1.1 constant_dynamic-slice_fusion
  67.4 0.5 broadcast.76
  67.9 0.7 reduce.5
  68.5 0.7 reshape.96
  69.2 3.3 %all-to-all-start.2 = ((bf16[4,2,192]{2,1,0:T(2,128)(2,1)}), bf16[4,2,192]{2,1,0:T(2,128)(2,1)S(1)}, u32[]{:S(2)}, u32[]{:S(2)}) async-start(bf16[4,2,192]{2,1,0:T(2,128)(2,1)} %reshape.96), calls=%async_computation.2 | async-start | bytes 8192 | tf_op jit(solution)/shard_map/all_to_all | solution.py:70
  72.6 0.4 fusion
  73.0 26.7 %all-gather.2.cloned.1.call-done = bf16[2,2048,512]{1,2,0:T(8,128)(2,1)} async-done(((bf16[2,2048,128]{1,2,0:T(8,128)(2,1)}), bf16[2,2048,512]{1,2,0:T(8,128)(2,1)}) %all-gather.2.cloned.1.call-update) | async-done | bytes 4194320 | tf_op jit(solution)/shard_map/all_gather | solution.py:56
  99.7 4.6 %fusion.10 = f32[2,384,512]{1,2,0:T(8,128)S(1)} fusion(bf16[2,2048,512]{1,2,0:T(8,128)(2,1)} %all-gather.2.cloned.1.call-done, bf16[1,384,2048]{2,1,0:T(8,128)(2,1)S(1)} %copy-done, f32[2048]{0:T(1024)S(1)} %copy-done.7, f32[384]{0:T(512)S(1)} %add_rsqrt_fusion.1), kind=kOutput, calls=%fused_computation.12 | convolution fusion | flops 1613758464 | bytes 7349760 | tf_op jit(solution)/shard_map/rd,kdc->krc/dot_general | solution.py:53
  104.4 0.3 copy.27
  104.7 0.2 copy-done.4
  104.9 1.0 multiply_convert_fusion
  106.0 3.6 %all-to-all-start = ((bf16[384,4,128]{2,0,1:T(8,128)(2,1)}), bf16[384,4,128]{2,0,1:T(8,128)(2,1)S(1)}, u32[]{:S(2)}, u32[]{:S(2)}) async-start(bf16[384,4,128]{2,0,1:T(8,128)(2,1)} %multiply_convert_fusion), calls=%async_computation | async-start | bytes 786432 | tf_op jit(solution)/shard_map/all_to_all | solution.py:68
  109.8 0.9 copy.28
  110.7 6.3 %all-to-all-done = bf16[384,4,128]{2,0,1:T(8,128)(2,1)S(1)} async-done(((bf16[384,4,128]{2,0,1:T(8,128)(2,1)}), bf16[384,4,128]{2,0,1:T(8,128)(2,1)S(1)}, u32[]{:S(2)}, u32[]{:S(2)}) %all-to-all-start) | async-done | bytes 393248 | tf_op jit(solution)/shard_map/all_to_all | solution.py:68
  116.9 3.5 %all-to-all-start.1 = ((bf16[384,4,128]{2,0,1:T(8,128)(2,1)}), bf16[384,4,128]{2,0,1:T(8,128)(2,1)S(1)}, u32[]{:S(2)}, u32[]{:S(2)}) async-start(bf16[384,4,128]{2,0,1:T(8,128)(2,1)} %copy.28), calls=%async_computation.1 | async-start | bytes 786432 | tf_op jit(solution)/shard_map/all_to_all | solution.py:69
  120.4 0.3 fusion.17
  120.7 5.0 %reduce-window.6 = f32[4,12,128]{2,1,0:T(8,128)S(1)} reduce-window(f32[4,12,128]{2,1,0:T(8,128)S(1)} %reshape.89, f32[]{:T(128)} %constant.50.clone.1), window={size=1x1x128 pad=0_0x0_0x0_127}, to_apply=%region_3.4 | reduce-window | flops 780288 | bytes 49156 | tf_op jit(solution)/shard_map/reduce-window
  126.1 1.7 %all-to-all-done.1 = bf16[384,4,128]{2,0,1:T(8,128)(2,1)S(1)} async-done(((bf16[384,4,128]{2,0,1:T(8,128)(2,1)}), bf16[384,4,128]{2,0,1:T(8,128)(2,1)S(1)}, u32[]{:S(2)}, u32[]{:S(2)}) %all-to-all-start.1) | async-done | bytes 393248 | tf_op jit(solution)/shard_map/all_to_all | solution.py:69
  127.8 0.3 multiply_reduce_fusion.1
  128.1 0.6 fusion.25
  128.8 0.7 copy.54
  129.5 0.7 copy.55
  (58 shorter events, 1.2 us)
Async XLA Ops:
  7.2 92.5 %all-gather.2.cloned.1.call-start = ((), (), s32[]{:S(2)}) async-start(), calls=%async_computation.3 | async-start | bytes 5242880 | tf_op jit(solution)/shard_map/all_gather | solution.py:56
  9.1 9.6 %collective-permute-start = (bf16[2,256,128]{1,2,0:T(8,128)(2,1)S(1)}, bf16[2,256,128]{1,2,0:T(8,128)(2,1)S(1)}, u32[]{:S(2)}, u32[]{:S(2)}) collective-permute-start(bf16[2,256,128]{1,2,0:T(8,128)(2,1)S(1)} %pad_maximum_fusion), channel_id=1, source_target_pairs={{0,4},{4,8},{8,12},{12,16},{16,20},{20,24},{24,28},{28,0},{1,5},{5... | collective-permute-start | bytes 393224 | tf_op jit(solution)/shard_map/ppermute | solution.py:17
  18.7 7.7 %collective-permute-start.1 = (bf16[2,256,128]{1,2,0:T(8,128)(2,1)S(1)}, bf16[2,256,128]{1,2,0:T(8,128)(2,1)S(1)}, u32[]{:S(2)}, u32[]{:S(2)}) collective-permute-start(bf16[2,256,128]{1,2,0:T(8,128)(2,1)S(1)} %collective-permute-done), channel_id=1, source_target_pairs={{0,4},{4,8},{8,12},{12,16},{16,20},{20,24},{24,28},{28,0},{1,5},{5... | collective-permute-start | bytes 393224 | tf_op jit(solution)/shard_map/ppermute | solution.py:17
  26.3 7.7 %collective-permute-start.2 = (bf16[2,256,128]{1,2,0:T(8,128)(2,1)S(1)}, bf16[2,256,128]{1,2,0:T(8,128)(2,1)S(1)}, u32[]{:S(2)}, u32[]{:S(2)}) collective-permute-start(bf16[2,256,128]{1,2,0:T(8,128)(2,1)S(1)} %collective-permute-done.1), channel_id=1, source_target_pairs={{0,4},{4,8},{8,12},{12,16},{16,20},{20,24},{24,28},{28,0},{1,5},{5... | collective-permute-start | bytes 393224 | tf_op jit(solution)/shard_map/ppermute | solution.py:17
  34.0 7.7 %collective-permute-start.3 = (bf16[2,256,128]{1,2,0:T(8,128)(2,1)S(1)}, bf16[2,256,128]{1,2,0:T(8,128)(2,1)S(1)}, u32[]{:S(2)}, u32[]{:S(2)}) collective-permute-start(bf16[2,256,128]{1,2,0:T(8,128)(2,1)S(1)} %collective-permute-done.2), channel_id=1, source_target_pairs={{0,4},{4,8},{8,12},{12,16},{16,20},{20,24},{24,28},{28,0},{1,5},{5... | collective-permute-start | bytes 393224 | tf_op jit(solution)/shard_map/ppermute | solution.py:17
  41.7 7.7 %collective-permute-start.4 = (bf16[2,256,128]{1,2,0:T(8,128)(2,1)S(1)}, bf16[2,256,128]{1,2,0:T(8,128)(2,1)S(1)}, u32[]{:S(2)}, u32[]{:S(2)}) collective-permute-start(bf16[2,256,128]{1,2,0:T(8,128)(2,1)S(1)} %collective-permute-done.3), channel_id=1, source_target_pairs={{0,4},{4,8},{8,12},{12,16},{16,20},{20,24},{24,28},{28,0},{1,5},{5... | collective-permute-start | bytes 393224 | tf_op jit(solution)/shard_map/ppermute | solution.py:17
  49.4 8.9 %collective-permute-start.5 = (bf16[2,256,128]{1,2,0:T(8,128)(2,1)S(1)}, bf16[2,256,128]{1,2,0:T(8,128)(2,1)S(1)}, u32[]{:S(2)}, u32[]{:S(2)}) collective-permute-start(bf16[2,256,128]{1,2,0:T(8,128)(2,1)S(1)} %collective-permute-done.4), channel_id=1, source_target_pairs={{0,4},{4,8},{8,12},{12,16},{16,20},{20,24},{24,28},{28,0},{1,5},{5... | collective-permute-start | bytes 393224 | tf_op jit(solution)/shard_map/ppermute | solution.py:17
  58.2 7.7 %collective-permute-start.6 = (bf16[2,256,128]{1,2,0:T(8,128)(2,1)S(1)}, bf16[2,256,128]{1,2,0:T(8,128)(2,1)S(1)}, u32[]{:S(2)}, u32[]{:S(2)}) collective-permute-start(bf16[2,256,128]{1,2,0:T(8,128)(2,1)S(1)} %collective-permute-done.5), channel_id=1, source_target_pairs={{0,4},{4,8},{8,12},{12,16},{16,20},{20,24},{24,28},{28,0},{1,5},{5... | collective-permute-start | bytes 393224 | tf_op jit(solution)/shard_map/ppermute | solution.py:17
  66.1 1.2 copy-start.2
  66.1 6.3 %copy-start.3 = (bf16[1,4,128]{2,1,0:T(4,128)(2,1)S(1)}, bf16[1,4,128]{2,1,0:T(4,128)(2,1)}, u32[]{:S(2)}) copy-start(bf16[1,4,128]{2,1,0:T(4,128)(2,1)} %param.15) | copy-start | bytes 3076
  66.2 6.5 %copy-start = (bf16[1,384,2048]{2,1,0:T(8,128)(2,1)S(1)}, bf16[1,384,2048]{2,1,0:T(8,128)(2,1)}, u32[]{:S(2)}) copy-start(bf16[1,384,2048]{2,1,0:T(8,128)(2,1)} %param.9) | copy-start | bytes 4718596
  66.2 33.4 %copy-start.7 = (f32[2048]{0:T(1024)S(1)}, f32[2048]{0:T(1024)}, u32[]{:S(2)}) copy-start(f32[2048]{0:T(1024)} %param.10) | copy-start | bytes 24580
  69.2 36.7 %all-to-all-start.2 = ((bf16[4,2,192]{2,1,0:T(2,128)(2,1)}), bf16[4,2,192]{2,1,0:T(2,128)(2,1)S(1)}, u32[]{:S(2)}, u32[]{:S(2)}) async-start(bf16[4,2,192]{2,1,0:T(2,128)(2,1)} %reshape.96), calls=%async_computation.2 | async-start | bytes 8192 | tf_op jit(solution)/shard_map/all_to_all | solution.py:70
  104.3 0.7 copy-start.4
  104.9 15.5 %copy-start.5 = (f32[128]{0:T(128)S(1)}, f32[128]{0:T(128)}, u32[]{:S(2)}) copy-start(f32[128]{0:T(128)} %param.16) | copy-start | bytes 1540
  106.0 22.2 %copy-start.6 = (f32[128]{0:T(128)S(1)}, f32[128]{0:T(128)}, u32[]{:S(2)}) copy-start(f32[128]{0:T(128)} %param.17) | copy-start | bytes 1540
  106.0 11.0 %all-to-all-start = ((bf16[384,4,128]{2,0,1:T(8,128)(2,1)}), bf16[384,4,128]{2,0,1:T(8,128)(2,1)S(1)}, u32[]{:S(2)}, u32[]{:S(2)}) async-start(bf16[384,4,128]{2,0,1:T(8,128)(2,1)} %multiply_convert_fusion), calls=%async_computation | async-start | bytes 786432 | tf_op jit(solution)/shard_map/all_to_all | solution.py:68
  109.7 19.8 %copy-start.1 = (bf16[4,1,384]{2,1,0:T(2,128)(2,1)}, bf16[4,1,384]{2,1,0:T(2,128)(2,1)S(1)}, u32[]{:S(2)}) copy-start(bf16[4,1,384]{2,1,0:T(2,128)(2,1)S(1)} %reshape.97) | copy-start | bytes 9220
  116.9 10.8 %all-to-all-start.1 = ((bf16[384,4,128]{2,0,1:T(8,128)(2,1)}), bf16[384,4,128]{2,0,1:T(8,128)(2,1)S(1)}, u32[]{:S(2)}, u32[]{:S(2)}) async-start(bf16[384,4,128]{2,0,1:T(8,128)(2,1)} %copy.28), calls=%async_computation.1 | async-start | bytes 786432 | tf_op jit(solution)/shard_map/all_to_all | solution.py:69
Sparse Core Ops, SparseCore 0:
  67.4 32.1 all-gather.1
